TPU v7x, 32 devices: a whole 2x2x4 slice. The times are simulated.
32 devices in a mesh: sp: 8 (over z, core), tp: 4 (over y, x).
Axes of the slice: x: 2, y: 2, z: 4, core: 2. Of those that a mesh axis runs over, the one named last changes fastest.
Arguments:
- moe_input: bfloat16 [2048, 2048], P('sp', 'tp'), may hold values from -6 to 6
- out_grad: bfloat16 [2048, 2048], P('sp', 'tp'), may hold values from -8 to 8
- routes: int32 [2048, 2], P('sp'), may hold values from 0 to 7, all different within a row; in each aligned block of 256 rows (0 to 255, 256 to 511, ...) at most 80 rows name the same one
- route_weight: float32 [2048, 2], P('sp'), may hold values from 0.2 to 1.5
- w_gate: bfloat16 [8, 2048, 2048], P('sp', None, 'tp'), may hold values from -0.125 to 0.125
- w_up: bfloat16 [8, 2048, 2048], P('sp', None, 'tp'), may hold values from -0.125 to 0.125
- w_down: bfloat16 [8, 2048, 2048], P('sp', 'tp'), may hold values from -0.125 to 0.125
- w_out: bfloat16 [2048, 2048], P(None, 'tp'), may hold values from -0.125 to 0.125
- queries: bfloat16 [2048, 1024], P('sp', 'tp'), may hold values from -6 to 6
- key_rows: bfloat16 [2048, 1024], P('sp', 'tp'), may hold values from -6 to 6
- value_rows: bfloat16 [2048, 2048], P('sp', 'tp'), may hold values from -6 to 6
- log_decay: float32 [2048, 1024], P('sp', 'tp'), may hold values from -1 to 0
Outputs:
- grad_gate: bfloat16 [8, 2048, 2048], P('sp', None, 'tp')
- grad_up: bfloat16 [8, 2048, 2048], P('sp', None, 'tp')
- grad_down: bfloat16 [8, 2048, 2048], P('sp', 'tp')
- grad_proj: float32 [2048, 2048], P('sp', 'tp')
- grad_queries: bfloat16 [2048, 1024], P('sp', 'tp')
- grad_keys: bfloat16 [2048, 1024], P('sp', 'tp')
- grad_values: bfloat16 [2048, 2048], P('sp', 'tp')
- grad_decay: float32 [2048, 1024], P('sp', 'tp')
Inputs may be any that keep to these rules, and one draw needn't show every extreme that they name: `routes`: A token's experts differ. Within each aligned block of 256 tokens no expert is named more than 80 times, and in some block one expert is named exactly 80 times.
All inputs are finite; a program needn't handle non-finite values.
Results may differ from a plain program's by a relative error of at most 0.025.
Values may be sent and summed in bfloat16 or wider, within the bound.
A program may use at most 64 MiB of HBM per device.

v0:
```python
import jax
import jax.numpy as jnp
from jax import lax
from jax.sharding import PartitionSpec as P

KEY_CHANNELS = 32
VAL_DIM = 64
TOP = 2
BLOCK = 64
PRECISE = lax.Precision.HIGHEST


def carried_in(value, axis, join, neutral, backward):
    count, mine = (lax.axis_size(axis), lax.axis_index(axis))
    pieces = jax.tree.map(lambda part: lax.all_gather(part, axis), value)
    if backward:
        pieces = jax.tree.map(lambda part: part[::-1], pieces)
        mine = count - 1 - mine
    subtotal = jax.tree.map(
        lambda part, zero: jnp.full_like(part, 0) + jnp.asarray(zero, part.dtype), value, neutral
    )

    def hop(position, subtotal):
        longer = join(subtotal, jax.tree.map(lambda part: part[position], pieces))
        return jax.tree.map(lambda new, old: jnp.where(position < mine, new, old), longer, subtotal)

    return lax.fori_loop(0, count - 1, hop, subtotal)


def mixer_pass(queries, key_rows, value_rows, log_decay, state_in):
    length = queries.shape[0]
    blocks = length // BLOCK
    nheads = state_in.shape[0]
    query_blocks = queries.reshape(blocks, BLOCK, nheads, KEY_CHANNELS)
    key_blocks = key_rows.reshape(blocks, BLOCK, nheads, KEY_CHANNELS) * KEY_CHANNELS ** (-0.5)
    value_blocks = value_rows.reshape(blocks, BLOCK, nheads, VAL_DIM)
    decays = log_decay.reshape(blocks, BLOCK, nheads, KEY_CHANNELS)
    cumulative = jnp.cumsum(decays, axis=1)
    closing = cumulative[:, -1]
    query_scaled = query_blocks * jnp.exp(cumulative)
    key_scaled = key_blocks * jnp.exp(-cumulative)
    causal = jnp.tril(jnp.ones((BLOCK, BLOCK), jnp.float32))
    scores = jnp.einsum("nthd,nshd->nhts", query_scaled, key_scaled, precision=PRECISE) * causal
    within = jnp.einsum("nhts,nshv->nthv", scores, value_blocks, precision=PRECISE)
    key_tail = key_blocks * jnp.exp(closing[:, None] - cumulative)
    additions = jnp.einsum("nshd,nshv->nhdv", key_tail, value_blocks, precision=PRECISE)

    def advance(state_now, pieces):
        return (jnp.exp(pieces[0])[..., None] * state_now + pieces[1], state_now)

    state_out, entering = lax.scan(advance, state_in, (closing, additions))
    carried = jnp.einsum("nthd,nhdv->nthv", query_scaled, entering, precision=PRECISE)
    return (within + carried).reshape(length, nheads * VAL_DIM)


def carry_terms(key_full, value_full, decay_full):
    length = key_full.shape[0]
    blocks = length // BLOCK
    nheads = key_full.shape[1] // KEY_CHANNELS
    key_blocks = key_full.reshape(blocks, BLOCK, nheads, KEY_CHANNELS) * KEY_CHANNELS ** (-0.5)
    value_blocks = value_full.reshape(blocks, BLOCK, nheads, VAL_DIM)
    cumulative = jnp.cumsum(decay_full.reshape(blocks, BLOCK, nheads, KEY_CHANNELS), axis=1)
    closing = cumulative[:, -1]
    key_tail = key_blocks * jnp.exp(closing[:, None] - cumulative)
    additions = jnp.einsum("nshd,nshv->nhdv", key_tail, value_blocks, precision=PRECISE)
    log_total = jnp.sum(closing, axis=0)
    remaining = log_total[None] - jnp.cumsum(closing, axis=0)
    increment = jnp.einsum("nhd,nhdv->hdv", jnp.exp(remaining), additions, precision=PRECISE)
    return (log_total, increment)


def chain_step(earlier, latter):
    return (earlier[0] + latter[0], jnp.exp(latter[0])[..., None] * earlier[1] + latter[1])


def body(
    moe_input,
    out_grad,
    routes,
    route_weight,
    w_gate,
    w_up,
    w_down,
    w_out,
    queries,
    key_rows,
    value_rows,
    log_decay,
):
    sp_count = lax.axis_size("sp")
    token_count = out_grad.shape[0]
    pair_count = token_count * TOP
    capacity = 5 * token_count * TOP // (4 * sp_count)
    query_full = queries.astype(jnp.float32)
    key_full = key_rows.astype(jnp.float32)
    value_full = value_rows.astype(jnp.float32)
    (log_total, increment), pull_carry = jax.vjp(carry_terms, key_full, value_full, log_decay)
    state_in = carried_in(
        (log_total, increment),
        "sp",
        chain_step,
        (jnp.zeros_like(log_total), jnp.zeros_like(increment)),
        False,
    )[1]
    mixer_raw, pull_mixer = jax.vjp(
        mixer_pass, query_full, key_full, value_full, log_decay, state_in
    )
    mixer_out = mixer_raw.astype(jnp.bfloat16)
    flat_routes = routes.reshape(pair_count)
    onehot = (flat_routes[:, None] == jnp.arange(sp_count, dtype=jnp.int32)[None, :]).astype(
        jnp.int32
    )
    position = jnp.sum((jnp.cumsum(onehot, axis=0) - onehot) * onehot, axis=1)
    pair_slot = flat_routes * capacity + position
    slot_pair = (
        jnp.full((sp_count * capacity,), pair_count, jnp.int32)
        .at[pair_slot]
        .set(jnp.arange(pair_count, dtype=jnp.int32))
    )
    slot_token = slot_pair // TOP
    row_total = sp_count * capacity
    columns = out_grad.shape[1]
    weighted = (route_weight[:, :, None] * out_grad[:, None, :].astype(jnp.float32)).astype(
        jnp.bfloat16
    )
    weighted_pad = jnp.concatenate(
        [weighted.reshape(pair_count, columns), jnp.zeros((1, columns), jnp.bfloat16)], axis=0
    )
    inputs_pad = jnp.concatenate([moe_input, jnp.zeros((1, columns), jnp.bfloat16)], axis=0)
    send_in = jnp.take(inputs_pad, slot_token, axis=0).reshape(sp_count, capacity, columns)
    send_grad = jnp.take(weighted_pad, slot_pair, axis=0).reshape(sp_count, capacity, columns)
    send_in, send_grad = (send_in, send_grad)
    recv_in, recv_grad = (
        lax.all_to_all(send_in, "sp", split_axis=0, concat_axis=0, tiled=True),
        lax.all_to_all(send_grad, "sp", split_axis=0, concat_axis=0, tiled=True),
    )
    rows_in, rows_grad = (
        lax.all_gather(recv_in.reshape(row_total, -1), "tp", axis=1, tiled=True),
        lax.all_gather(recv_grad.reshape(row_total, -1), "tp", axis=1, tiled=True),
    )
    gate_weight = w_gate[0]
    up_weight = w_up[0]
    down_weight = w_down[0]
    gate_pre = jnp.dot(rows_in, gate_weight, preferred_element_type=jnp.float32)
    up_pre = jnp.dot(rows_in, up_weight, preferred_element_type=jnp.float32)
    sigmoid_gate = jax.nn.sigmoid(gate_pre)
    activated = gate_pre * sigmoid_gate
    hidden = (activated * up_pre).astype(jnp.bfloat16)
    hidden_grad = lax.dot_general(
        rows_grad, down_weight, (((1,), (1,)), ((), ())), preferred_element_type=jnp.float32
    )
    down_part = lax.dot_general(
        hidden, rows_grad, (((0,), (0,)), ((), ())), preferred_element_type=jnp.float32
    ).astype(jnp.bfloat16)
    gate_grad = (
        hidden_grad * up_pre * sigmoid_gate * (1.0 + gate_pre * (1.0 - sigmoid_gate))
    ).astype(jnp.bfloat16)
    up_grad = (hidden_grad * activated).astype(jnp.bfloat16)
    gate_part = lax.dot_general(
        rows_in, gate_grad, (((0,), (0,)), ((), ())), preferred_element_type=jnp.float32
    ).astype(jnp.bfloat16)
    up_part = lax.dot_general(
        rows_in, up_grad, (((0,), (0,)), ((), ())), preferred_element_type=jnp.float32
    ).astype(jnp.bfloat16)
    partial_value = lax.dot_general(
        gate_grad, gate_weight, (((1,), (1,)), ((), ())), preferred_element_type=jnp.float32
    )
    partial_value = partial_value + lax.dot_general(
        up_grad, up_weight, (((1,), (1,)), ((), ())), preferred_element_type=jnp.float32
    )
    row_part = lax.psum_scatter(
        partial_value.astype(jnp.bfloat16), "tp", scatter_dimension=1, tiled=True
    )
    back_rows = lax.all_to_all(
        row_part.reshape(sp_count, capacity, -1), "sp", split_axis=0, concat_axis=0, tiled=True
    ).reshape(row_total, -1)
    routed = jnp.sum(
        jnp.take(back_rows, pair_slot, axis=0).astype(jnp.float32).reshape(token_count, TOP, -1),
        axis=1,
    )
    residual_grad = (out_grad.astype(jnp.float32) + routed).astype(jnp.bfloat16)
    full_grad = lax.all_gather(residual_grad, "tp", axis=1, tiled=True)
    grad_proj = lax.psum_scatter(
        lax.dot_general(
            full_grad, mixer_out, (((0,), (0,)), ((), ())), preferred_element_type=jnp.float32
        ).astype(jnp.bfloat16),
        "sp",
        scatter_dimension=0,
        tiled=True,
    ).astype(jnp.float32)
    mixer_grad = jnp.dot(full_grad, w_out, preferred_element_type=jnp.float32)
    query_grad, key_grad, value_grad, decay_grad, state_grad = pull_mixer(mixer_grad)
    state_out_grad = carried_in(
        (log_total, state_grad),
        "sp",
        chain_step,
        (jnp.zeros_like(log_total), jnp.zeros_like(state_grad)),
        True,
    )[1]
    total_grad = jnp.exp(log_total) * jnp.sum(state_out_grad * state_in, axis=2)
    key_extra, value_extra, decay_extra = pull_carry((total_grad, state_out_grad))
    return (
        gate_part[None],
        up_part[None],
        down_part[None],
        grad_proj,
        query_grad.astype(jnp.bfloat16),
        (key_grad + key_extra).astype(jnp.bfloat16),
        (value_grad + value_extra).astype(jnp.bfloat16),
        decay_grad + decay_extra,
    )


def solution(mesh):
    in_specs = (
        P("sp", "tp"),
        P("sp", "tp"),
        P("sp", None),
        P("sp", None),
        P("sp", None, "tp"),
        P("sp", None, "tp"),
        P("sp", "tp", None),
        P(None, "tp"),
        P("sp", "tp"),
        P("sp", "tp"),
        P("sp", "tp"),
        P("sp", "tp"),
    )
    out_specs = (
        P("sp", None, "tp"),
        P("sp", None, "tp"),
        P("sp", "tp", None),
        P("sp", "tp"),
        P("sp", "tp"),
        P("sp", "tp"),
        P("sp", "tp"),
        P("sp", "tp"),
    )
    return jax.shard_map(body, mesh=mesh, in_specs=in_specs, out_specs=out_specs, check_vma=False)
```

profile of v0, /device:TPU:0, one launch (start us, length us, event | category | flops | bytes accessed | tf_op | source)
XLA Modules:
  0.0 410.4 jit_solution(14217362036748022045)
XLA Ops:
  11.5 2.4 scatter_custom_fusion
  15.1 2.8 gather_fusion
  18.1 24.4 %all_to_all.15 = bf16[8,80,512]{2,1,0:T(8,128)(2,1)} all-to-all(bf16[8,80,512]{2,1,0:T(8,128)(2,1)S(1)} %broadcast_select_fusion.2), channel_id=1, replica_groups=mesh['sp'=8,'tp'=4] {'sp'}, dimensions={0} | all-to-all | bytes 1310720 | tf_op jit(solution)/shard_map/all_to_all | solution.py:134
  46.3 2.8 gather_fusion.1
  49.3 21.2 %all_to_all.16 = bf16[8,80,512]{2,1,0:T(8,128)(2,1)} all-to-all(bf16[8,80,512]{2,1,0:T(8,128)(2,1)S(1)} %broadcast_select_fusion.1), channel_id=1, replica_groups=mesh['sp'=8,'tp'=4] {'sp'}, dimensions={0} | all-to-all | bytes 1310720 | tf_op jit(solution)/shard_map/all_to_all | solution.py:135
  71.1 9.8 %all-gather.7.cloned.1.call-done = bf16[640,2048]{1,0:T(8,128)(2,1)} async-done(((bf16[640,512]{1,0:T(8,128)(2,1)}), bf16[640,2048]{1,0:T(8,128)(2,1)}) %all-gather.7.cloned.1.call-update) | async-done | bytes 2621456 | tf_op jit(solution)/shard_map/all_gather | solution.py:138
  81.0 3.4 fusion.11
  84.4 2.6 fusion.14
  87.0 35.2 %all-gather.9.cloned.1.call-done = bf16[640,2048]{1,0:T(8,128)(2,1)} async-done(((bf16[640,512]{1,0:T(8,128)(2,1)}), bf16[640,2048]{1,0:T(8,128)(2,1)}) %all-gather.9.cloned.1.call-update) | async-done | bytes 2621456 | tf_op jit(solution)/shard_map/all_gather | solution.py:139
  122.2 4.6 %multiply_convert_fusion.1 = (bf16[640,512]{1,0:T(8,128)(2,1)S(1)}, bf16[640,512]{1,0:T(8,128)(2,1)S(1)}) fusion(f32[640,512]{1,0:T(8,128)S(1)} %fusion.11, f32[640,512]{1,0:T(8,128)} %fusion.14, bf16[640,2048]{1,0:T(8,128)(2,1)} %all-gather.9.cloned.1.call-done, bf16[1,512,2048]{2,1,0:T(8,128)(2,1)} %param.26), kind=kOutput, calls=%fused_computation.48 | convolution fusion | flops 1346437120 | bytes 8650752 | tf_op jit(solution)/shard_map/dot_general | solution.py:149
  128.9 3.1 add_convert_fusion
  133.6 25.9 %fusion.66 = f32[4,64,8,32]{3,2,1,0:T(8,128)S(1)} fusion(f32[4,64,8,32]{3,2,1,0:T(8,128)S(1)} %reshape.284), kind=kOutput, calls=%fused_computation.146 | output fusion | flops 4128768 | bytes 524288 | tf_op jit(solution)/shard_map/jvp(jit(cumsum))/reduce_window_sum | solution.py:38
  162.7 14.1 %all-gather = f32[64,32]{1,0:T(8,128)S(1)} all-gather(f32[8,32]{1,0:T(8,128)S(1)} %get-tuple-element.558), channel_id=2, replica_groups=mesh['sp'=8,'tp'=4] {'sp'}, dimensions={0}, use_global_device_ids=true | all-gather | bytes 9216 | tf_op jit(solution)/shard_map/all_gather | solution.py:15
  180.5 16.9 %all-gather.1 = f32[64,32,64]{2,1,0:T(8,128)S(1)} all-gather(f32[8,32,64]{2,1,0:T(8,128)S(1)} %bitcast.213), channel_id=3, replica_groups=mesh['sp'=8,'tp'=4] {'sp'}, dimensions={0}, use_global_device_ids=true | all-gather | bytes 589824 | tf_op jit(solution)/shard_map/all_gather | solution.py:15
  199.2 5.0 %all-to-all-start.2 = ((bf16[8,80,512]{2,1,0:T(8,128)(2,1)}), bf16[8,80,512]{2,1,0:T(8,128)(2,1)S(1)}, u32[]{:S(2)}, u32[]{:S(2)}) async-start(bf16[8,80,512]{2,1,0:T(8,128)(2,1)} %bitcast.208), calls=%async_computation.3 | async-start | bytes 1310720 | tf_op jit(solution)/shard_map/all_to_all | solution.py:174
  204.6 6.7 %while.63 = (s32[]{:T(128)}, f32[8,32,64]{2,1,0:T(8,128)S(1)}, f32[4,8,32,64]{3,2,1,0:T(8,128)S(1)}, f32[4,8,32]{2,1,0:T(8,128)S(1)}, f32[4,8,32,1]{2,1,3,0:T(8,...) while((s32[]{:T(128)}, f32[8,32,64]{2,1,0:T(8,128)S(1)}, ...), condition=%wide.region_12.13_spmd, body=%wide.region_11.12_spmd.sunk | while | flops 32770 | bytes 477293 | solution.py:51
  226.6 2.4 convert_reduce_fusion
  230.8 3.1 fusion.20
  234.6 5.0 %fusion.6 = bf16[1,2048,512]{2,1,0:T(8,128)(2,1)} fusion(bf16[640,2048]{1,0:T(8,128)(2,1)} %all-gather.7.cloned.1.call-done, bf16[640,512]{1,0:T(8,128)(2,1)S(1)} %copy-done.28), kind=kOutput, calls=%fused_computation.28 | convolution fusion | flops 1343225856 | bytes 5373952 | tf_op jit(solution)/shard_map/dot_general | solution.py:159
  239.7 3.2 fusion.7
  242.9 3.3 fusion.8
  246.2 11.6 %all-gather.11.cloned.1.call-done = bf16[256,2048]{1,0:T(8,128)(2,1)} async-done(((bf16[256,512]{1,0:T(8,128)(2,1)}), bf16[256,2048]{1,0:T(8,128)(2,1)}) %all-gather.11.cloned.1.call-update) | async-done | bytes 1048592 | tf_op jit(solution)/shard_map/all_gather | solution.py:182
  257.7 3.3 convolution_convert_fusion
  262.2 2.3 fusion.69
  267.3 2.5 fusion.27
  270.8 12.7 %while.65 = (s32[]{:T(128)}, f32[8,32,64]{2,1,0:T(8,128)S(1)}, f32[4,8,32]{2,1,0:T(8,128)S(1)}, f32[4,8,32,64]{3,2,1,0:T(8,128)}, f32[4,8,32,64]{3,2,1,0:T(8,128...) while((s32[]{:T(128)}, f32[8,32,64]{2,1,0:T(8,128)S(1)}, ...), condition=%wide.region_16.17_spmd.clone, body=%wide.region_14.16_spmd.clone.sunk | while | flops 98308 | bytes 472220 | solution.py:51
  283.5 2.8 fusion.41
  286.3 19.8 %all-gather.2 = f32[64,32,64]{2,1,0:T(8,128)} all-gather(f32[8,32,64]{2,1,0:T(8,128)S(1)} %get-tuple-element.402), channel_id=4, replica_groups=mesh['sp'=8,'tp'=4] {'sp'}, dimensions={0}, use_global_device_ids=true | all-gather | bytes 589824 | tf_op jit(solution)/shard_map/all_gather | solution.py:15
  308.3 12.5 %while.66 = (s32[]{:T(128)}, f32[8,32,64]{2,1,0:T(8,128)S(1)}, s32[]{:T(128)}, f32[8,8,32]{2,1,0:T(8,128)}, f32[8,8,32,64]{3,2,1,0:T(8,128)}, /*index=5*/s32[]{:T(128)}, s32[]{:T(128)}) while((s32[]{:T(128)}, f32[8,32,64]{2,1,0:T(8,128)S(1)}, s32[]{:T(128)}, f32[8,8,32]{2,1,0:T(8,128)}, f32[8,8,32,64]{3,2,1,0:T(8,128)}, ...), condition=%wide.region_18.19_spmd.clone, body=%wide.region_17.18_spmd.clone.sunk | while | flops 65540 | bytes 199793 | solution.py:27
  327.1 2.9 pad_add_fusion.1
  349.0 25.7 %fusion.67 = f32[4,64,8,32]{3,2,1,0:T(8,128)S(1)} fusion(f32[4,64,8,32]{3,2,1,0:T(8,128)S(1)} %copy.145), kind=kOutput, calls=%fused_computation.147 | output fusion | flops 4128768 | bytes 524288 | tf_op jit(solution)/shard_map/transpose(jvp(jit(cumsum)))/reduce_window_sum | solution.py:38
  374.7 25.8 %fusion.68 = f32[4,64,8,32]{3,2,1,0:T(8,128)S(1)} fusion(f32[4,64,8,32]{3,2,1,0:T(8,128)S(1)} %copy-done.16), kind=kOutput, calls=%fused_computation.148 | output fusion | flops 4128768 | bytes 524288 | tf_op jit(solution)/shard_map/transpose(jvp(jit(cumsum)))/reduce_window_sum | solution.py:62
  (281 shorter events, 107.8 us)
Async XLA Ops:
  7.2 73.8 %copy-start = (bf16[1,2048,512]{2,1,0:T(8,128)(2,1)S(1)}, bf16[1,2048,512]{2,1,0:T(8,128)(2,1)}, u32[]{:S(2)}) copy-start(bf16[1,2048,512]{2,1,0:T(8,128)(2,1)} %param.24) | copy-start | bytes 6291460
  7.2 73.8 %all-gather.7.cloned.1.call-start = ((), (), s32[]{:S(2)}) async-start(), calls=%async_computation.5 | async-start | bytes 3276800 | tf_op jit(solution)/shard_map/all_gather | solution.py:138
  17.9 24.6 %copy-start.26 = (bf16[256,512]{1,0:T(8,128)(2,1)S(1)}, bf16[256,512]{1,0:T(8,128)(2,1)}, u32[]{:S(2)}) copy-start(bf16[256,512]{1,0:T(8,128)(2,1)} %param.21) | copy-start | bytes 786436
  42.5 79.7 %all-gather.9.cloned.1.call-start = ((), (), s32[]{:S(2)}) async-start(), calls=%async_computation.6 | async-start | bytes 3276800 | tf_op jit(solution)/shard_map/all_gather | solution.py:139
  70.6 128.7 %reduce-scatter.3.cloned.1.call-start = ((), (), s32[]{:S(2)}) async-start(), calls=%async_computation.7 | async-start | bytes 3276800 | tf_op jit(solution)/shard_map/reduce_scatter | solution.py:171
  81.0 3.4 copy-start.20
  81.0 3.4 copy-start.47
  84.4 37.8 %copy-start.50 = (f32[640,512]{1,0:T(8,128)}, f32[640,512]{1,0:T(8,128)S(1)}, u32[]{:S(2)}) copy-start(f32[640,512]{1,0:T(8,128)S(1)} %fusion.11) | copy-start | bytes 3932164
  133.6 26.3 %copy-start.39 = (bf16[256,256]{1,0:T(8,128)(2,1)S(1)}, bf16[256,256]{1,0:T(8,128)(2,1)}, u32[]{:S(2)}) copy-start(bf16[256,256]{1,0:T(8,128)(2,1)} %param.28) | copy-start | bytes 393220
  159.9 59.2 %copy-start.2 = (f32[4,64,8,32]{1,3,2,0:T(8,128)}, f32[4,64,8,32]{1,3,2,0:T(8,128)S(1)}, u32[]{:S(2)}) copy-start(f32[4,64,8,32]{1,3,2,0:T(8,128)S(1)} %copy.122) | copy-start | bytes 786436
  160.7 17.6 %copy-start.12 = (f32[4,64,8,32]{1,0,3,2:T(4,128)}, f32[4,64,8,32]{1,0,3,2:T(4,128)S(1)}, u32[]{:S(2)}) copy-start(f32[4,64,8,32]{1,0,3,2:T(4,128)S(1)} %reshape.242) | copy-start | bytes 786436
  161.8 16.6 %copy-start.41 = (f32[8,32]{1,0:T(8,128)}, f32[8,32]{1,0:T(8,128)S(1)}, u32[]{:S(2)}) copy-start(f32[8,32]{1,0:T(8,128)S(1)} %get-tuple-element.558) | copy-start | bytes 3076
  162.5 15.8 %copy-start.31 = (f32[4,8,32]{2,1,0:T(8,128)}, f32[4,8,32]{2,1,0:T(8,128)S(1)}, u32[]{:S(2)}) copy-start(f32[4,8,32]{2,1,0:T(8,128)S(1)} %fusion.25) | copy-start | bytes 12292
  199.2 5.1 %copy-start.10 = (f32[8,32,64]{2,1,0:T(8,128)}, f32[8,32,64]{2,1,0:T(8,128)S(1)}, u32[]{:S(2)}) copy-start(f32[8,32,64]{2,1,0:T(8,128)S(1)} %get-tuple-element.750) | copy-start | bytes 196612
  199.2 25.0 %all-to-all-start.2 = ((bf16[8,80,512]{2,1,0:T(8,128)(2,1)}), bf16[8,80,512]{2,1,0:T(8,128)(2,1)S(1)}, u32[]{:S(2)}, u32[]{:S(2)}) async-start(bf16[8,80,512]{2,1,0:T(8,128)(2,1)} %bitcast.208), calls=%async_computation.3 | async-start | bytes 1310720 | tf_op jit(solution)/shard_map/all_to_all | solution.py:174
  204.3 7.0 %copy-start.44 = (s32[512]{0:T(512)S(1)}, s32[512]{0:T(512)}, u32[]{:S(2)}) copy-start(s32[512]{0:T(512)} %copy-done.43) | copy-start | bytes 6148
  204.3 53.4 %all-gather.11.cloned.1.call-start = ((), (), s32[]{:S(2)}) async-start(), calls=%async_computation.8 | async-start | bytes 1310720 | tf_op jit(solution)/shard_map/all_gather | solution.py:182
  211.3 19.5 %copy-start.4 = (f32[4,8,32,64]{3,2,1,0:T(8,128)}, f32[4,8,32,64]{3,2,1,0:T(8,128)S(1)}, u32[]{:S(2)}) copy-start(f32[4,8,32,64]{3,2,1,0:T(8,128)S(1)} %get-tuple-element.779) | copy-start | bytes 786436
  230.7 170.9 %reduce-scatter.5.cloned.1.call-start = ((), (), s32[]{:S(2)}) async-start(), calls=%async_computation.9 | async-start | bytes 2359296 | tf_op jit(solution)/shard_map/reduce_scatter | solution.py:183
  230.8 3.8 copy-start.28
  234.6 5.1 %copy-start.30 = (bf16[640,512]{1,0:T(8,128)(2,1)S(1)}, bf16[640,512]{1,0:T(8,128)(2,1)}, u32[]{:S(2)}) copy-start(bf16[640,512]{1,0:T(8,128)(2,1)} %copy-done.29) | copy-start | bytes 1966084
  234.6 5.1 %copy-start.48 = (bf16[640,2048]{1,0:T(8,128)(2,1)S(1)}, bf16[640,2048]{1,0:T(8,128)(2,1)}, u32[]{:S(2)}) copy-start(bf16[640,2048]{1,0:T(8,128)(2,1)} %all-gather.7.cloned.1.call-done) | copy-start | bytes 7864324
  270.8 12.7 %copy-start.3 = (f32[4,64,8,32]{1,3,2,0:T(8,128)S(1)}, f32[4,64,8,32]{1,3,2,0:T(8,128)}, u32[]{:S(2)}) copy-start(f32[4,64,8,32]{1,3,2,0:T(8,128)} %copy-done.2) | copy-start | bytes 786436
  306.0 15.8 %copy-start.32 = (f32[4,8,32]{2,1,0:T(8,128)S(1)}, f32[4,8,32]{2,1,0:T(8,128)}, u32[]{:S(2)}) copy-start(f32[4,8,32]{2,1,0:T(8,128)} %copy-done.31) | copy-start | bytes 12292
  320.8 4.2 %copy-start.34 = (f32[64,64]{1,0:T(8,128)S(1)}, f32[64,64]{1,0:T(8,128)}, u32[]{:S(2)}) copy-start(f32[64,64]{1,0:T(8,128)} %copy-done.33) | copy-start | bytes 49156
  330.0 6.8 %copy-start.9 = (f32[4,64,8,32]{1,3,2,0:T(8,128)S(1)}, f32[4,64,8,32]{1,3,2,0:T(8,128)}, u32[]{:S(2)}) copy-start(f32[4,64,8,32]{1,3,2,0:T(8,128)} %copy-done.8) | copy-start | bytes 786436
  330.0 6.8 %copy-start.14 = (f32[4,8,32,64]{3,2,1,0:T(8,128)S(1)}, f32[4,8,32,64]{3,2,1,0:T(8,128)}, u32[]{:S(2)}) copy-start(f32[4,8,32,64]{3,2,1,0:T(8,128)} %get-tuple-element.401) | copy-start | bytes 786436
  330.9 7.8 %copy-start.7 = (f32[4,8,64,64]{3,2,1,0:T(8,128)S(1)}, f32[4,8,64,64]{3,2,1,0:T(8,128)}, u32[]{:S(2)}) copy-start(f32[4,8,64,64]{3,2,1,0:T(8,128)} %copy-done.6) | copy-start | bytes 1572868
  339.9 3.6 copy-start.23
  343.9 3.5 copy-start.22
  349.0 25.7 %copy-start.16 = (f32[4,64,8,32]{3,2,1,0:T(8,128)S(1)}, f32[4,64,8,32]{3,2,1,0:T(8,128)}, u32[]{:S(2)}) copy-start(f32[4,64,8,32]{3,2,1,0:T(8,128)} %copy.149) | copy-start | bytes 786436
  374.7 28.7 %copy-start.1 = (bf16[1,2048,512]{2,1,0:T(8,128)(2,1)S(1)}, bf16[1,2048,512]{2,1,0:T(8,128)(2,1)}, u32[]{:S(2)}) copy-start(bf16[1,2048,512]{2,1,0:T(8,128)(2,1)} %param.24) | copy-start | bytes 6291460
  (27 other events, 50.2 us)
Sparse Core Ops, SparseCore 0:
  42.6 38.3 all-gather.6
  82.8 39.3 all-gather.8
  132.2 39.5 reduce-scatter.2
  230.8 26.8 all-gather.10
  261.2 36.9 reduce-scatter.4
where the time goes:
time: 417 us; the launch traced here: 410 us
  other arithmetic  115 us (28%)
  blocking collectives  96.4 us (23%)
  matrix products  62.1 us (15%)
  local copies, waits for them, and re-layouts  58.6 us (14%)
  waiting for transfers between devices  56.7 us (14%)
  between operations  15.2 us (4%)
  starting transfers between devices  5.94 us (1%)
    another operation x2, other arithmetic, mixer_pass(): cumulative = jnp.cumsum(decays, axis=1)  51.5 us
    all_gather x3, blocking collectives, carried_in(): pieces = jax.tree.map(lambda part: lax.all_gather(part, axis), value)  50.8 us
    all_gather x1, waiting for transfers between devices, body(): lax.all_gather(recv_grad.reshape(row_total, -1), 'tp', axis=1, tiled=True)  35.2 us
    another operation x1, other arithmetic, carry_terms(): jnp.cumsum(decay_full.reshape(blocks, BLOCK, nheads, KEY_CHANNELS), axis=1)  25.8 us
    all_to_all x1, blocking collectives, body(): lax.all_to_all(send_in, 'sp', split_axis=0, concat_axis=0, tiled=True)  24.4 us
    all_to_all x1, blocking collectives, body(): lax.all_to_all(send_grad, 'sp', split_axis=0, concat_axis=0, tiled=True)  21.2 us
    all_gather x1, waiting for transfers between devices, body(): full_grad = lax.all_gather(residual_grad, 'tp', axis=1, tiled=True)  11.6 us
    all_gather x1, waiting for transfers between devices, body(): lax.all_gather(recv_in.reshape(row_total, -1), 'tp', axis=1, tiled=True)  9.84 us
  transfers between devices with their start and end apart: 6, of which 3 were waited for; matrix products, arithmetic and copies ran while one was open for 48% of the time, Pallas kernels for 0%

commit v1 on v0

--- a/solution.py
+++ b/solution.py
@@ -136,7 +136,12 @@
     )
     rows_in, rows_grad = (
         lax.all_gather(recv_in.reshape(row_total, -1), "tp", axis=1, tiled=True),
-        lax.all_gather(recv_grad.reshape(row_total, -1), "tp", axis=1, tiled=True),
+        jnp.concatenate(
+            lax.all_to_all(
+                jnp.stack([recv_grad.reshape(row_total, -1)] * lax.axis_size("tp")), "tp", 0, 0
+            ),
+            axis=1,
+        ),
     )
     gate_weight = w_gate[0]
     up_weight = w_up[0]

time: 417 us -> 404 us (0.969)
  waiting for transfers between devices: 56.7 us -> 36 us
  starting transfers between devices: 5.94 us -> 10.3 us
    all_gather x1 -> x0, waiting for transfers between devices: 35.2 us -> none  [body(): lax.all_gather(recv_grad.reshape(row_total, -1), 'tp', axis=1, tiled=True)]
    all_gather x1, waiting for transfers between devices: 9.84 us -> 19.9 us  [body(): lax.all_gather(recv_in.reshape(row_total, -1), 'tp', axis=1, tiled=True)]
    all_to_all x0 -> x1, waiting for transfers between devices: none -> 6.12 us  [body(): lax.all_to_all(jnp.stack([recv_grad.reshape(row_total, -1)] * lax.axis_si...]
    all_to_all x0 -> x1, starting transfers between devices: none -> 4.56 us  [body(): lax.all_to_all(jnp.stack([recv_grad.reshape(row_total, -1)] * lax.axis_si...]
    unnamed x111 -> x109, local copies, waits for them, and re-layouts: 9.22 us -> 9.23 us
  transfers between devices with their start and end apart: 6 -> 6, of which waited for: 3 -> 3; matrix products, arithmetic and copies ran while one was open for 48% -> 51% of each run, Pallas kernels for 0% -> 0%
where the time goes in v1:
time: 404 us; the launch traced here: 397 us
  other arithmetic  115 us (28%)
  blocking collectives  95.8 us (24%)
  matrix products  63.8 us (16%)
  local copies, waits for them, and re-layouts  60.6 us (15%)
  waiting for transfers between devices  36 us (9%)
  between operations  15.2 us (4%)
  starting transfers between devices  10.3 us (3%)
    another operation x2, other arithmetic, mixer_pass(): cumulative = jnp.cumsum(decays, axis=1)  51.5 us
    all_gather x3, blocking collectives, carried_in(): pieces = jax.tree.map(lambda part: lax.all_gather(part, axis), value)  50.9 us
    another operation x1, other arithmetic, carry_terms(): jnp.cumsum(decay_full.reshape(blocks, BLOCK, nheads, KEY_CHANNELS), axis=1)  25.8 us
    all_to_all x1, blocking collectives, body(): lax.all_to_all(send_in, 'sp', split_axis=0, concat_axis=0, tiled=True)  24.4 us
    all_to_all x1, blocking collectives, body(): lax.all_to_all(send_grad, 'sp', split_axis=0, concat_axis=0, tiled=True)  20.5 us
    all_gather x1, waiting for transfers between devices, body(): lax.all_gather(recv_in.reshape(row_total, -1), 'tp', axis=1, tiled=True)  19.9 us
    all_gather x1, waiting for transfers between devices, body(): full_grad = lax.all_gather(residual_grad, 'tp', axis=1, tiled=True)  9.91 us
    unnamed x109, local copies, waits for them, and re-layouts  9.23 us
  transfers between devices with their start and end apart: 6, of which 3 were waited for; matrix products, arithmetic and copies ran while one was open for 51% of the time, Pallas kernels for 0%

profile of v1, /device:TPU:0, one launch (start us, length us, event | category | flops | bytes accessed | tf_op | source)
XLA Modules:
  0.0 397.1 jit_solution(12184053926959064230)
XLA Ops:
  11.5 2.4 scatter_custom_fusion
  15.1 2.8 gather_fusion
  18.1 24.4 %all_to_all.20 = bf16[8,80,512]{2,1,0:T(8,128)(2,1)} all-to-all(bf16[8,80,512]{2,1,0:T(8,128)(2,1)S(1)} %broadcast_select_fusion.2), channel_id=1, replica_groups=mesh['sp'=8,'tp'=4] {'sp'}, dimensions={0} | all-to-all | bytes 1310720 | tf_op jit(solution)/shard_map/all_to_all | solution.py:134
  46.3 2.8 gather_fusion.1
  49.2 20.5 %all_to_all.21 = bf16[8,80,512]{2,1,0:T(8,128)(2,1)S(1)} all-to-all(bf16[8,80,512]{2,1,0:T(8,128)(2,1)S(1)} %broadcast_select_fusion.1), channel_id=1, replica_groups=mesh['sp'=8,'tp'=4] {'sp'}, dimensions={0} | all-to-all | bytes 1310720 | tf_op jit(solution)/shard_map/all_to_all | solution.py:135
  71.8 4.6 %all-to-all-start.2 = ((bf16[4,640,512]{1,2,0:T(8,128)(2,1)}), bf16[4,640,512]{1,2,0:T(8,128)(2,1)}, u32[]{:S(2)}, u32[]{:S(2)}) async-start(bf16[4,640,512]{1,2,0:T(8,128)(2,1)} %stack.3), calls=%async_computation.2 | async-start | bytes 5242880 | tf_op jit(solution)/shard_map/all_to_all | solution.py:140
  76.9 19.9 %all-gather.6.cloned.1.call-done = bf16[640,2048]{1,0:T(8,128)(2,1)} async-done(((bf16[640,512]{1,0:T(8,128)(2,1)}), bf16[640,2048]{1,0:T(8,128)(2,1)}) %all-gather.6.cloned.1.call-update) | async-done | bytes 2621456 | tf_op jit(solution)/shard_map/all_gather | solution.py:138
  96.8 3.4 fusion.11
  100.2 2.6 fusion.14
  102.8 6.1 %all-to-all-done.2 = bf16[4,640,512]{1,2,0:T(8,128)(2,1)} async-done(((bf16[4,640,512]{1,2,0:T(8,128)(2,1)}), bf16[4,640,512]{1,2,0:T(8,128)(2,1)}, u32[]{:S(2)}, u32[]{:S(2)}) %all-to-all-start.2) | async-done | bytes 2621472 | tf_op jit(solution)/shard_map/all_to_all | solution.py:140
  108.9 4.7 %multiply_convert_fusion.1 = (bf16[640,512]{1,0:T(8,128)(2,1)S(1)}, bf16[640,512]{1,0:T(8,128)(2,1)S(1)}) fusion(f32[640,512]{1,0:T(8,128)S(1)} %fusion.11, f32[640,512]{1,0:T(8,128)} %fusion.14, bf16[640,2048]{0,1:T(8,128)(2,1)} %bitcast.13, bf16[1,512,2048]{2,1,0:T(8,128)(2,1)} %param.26), kind=kOutput, calls=%fused_computation.48 | convolution fusion | flops 1346437120 | bytes 8650752 | tf_op jit(solution)/shard_map/dot_general | solution.py:154
  115.7 3.1 add_convert_fusion
  120.4 25.9 %fusion.66 = f32[4,64,8,32]{3,2,1,0:T(8,128)S(1)} fusion(f32[4,64,8,32]{3,2,1,0:T(8,128)S(1)} %reshape.290), kind=kOutput, calls=%fused_computation.146 | output fusion | flops 4128768 | bytes 524288 | tf_op jit(solution)/shard_map/jvp(jit(cumsum))/reduce_window_sum | solution.py:38
  149.4 14.1 %all-gather = f32[64,32]{1,0:T(8,128)S(1)} all-gather(f32[8,32]{1,0:T(8,128)S(1)} %get-tuple-element.558), channel_id=2, replica_groups=mesh['sp'=8,'tp'=4] {'sp'}, dimensions={0}, use_global_device_ids=true | all-gather | bytes 9216 | tf_op jit(solution)/shard_map/all_gather | solution.py:15
  167.2 17.0 %all-gather.1 = f32[64,32,64]{2,1,0:T(8,128)S(1)} all-gather(f32[8,32,64]{2,1,0:T(8,128)S(1)} %bitcast.216), channel_id=3, replica_groups=mesh['sp'=8,'tp'=4] {'sp'}, dimensions={0}, use_global_device_ids=true | all-gather | bytes 589824 | tf_op jit(solution)/shard_map/all_gather | solution.py:15
  186.2 5.0 %all-to-all-start.3 = ((bf16[8,80,512]{2,1,0:T(8,128)(2,1)}), bf16[8,80,512]{2,1,0:T(8,128)(2,1)S(1)}, u32[]{:S(2)}, u32[]{:S(2)}) async-start(bf16[8,80,512]{2,1,0:T(8,128)(2,1)} %bitcast.211), calls=%async_computation.4 | async-start | bytes 1310720 | tf_op jit(solution)/shard_map/all_to_all | solution.py:179
  191.3 6.7 %while.63 = (s32[]{:T(128)}, f32[8,32,64]{2,1,0:T(8,128)S(1)}, f32[4,8,32,64]{3,2,1,0:T(8,128)S(1)}, f32[4,8,32]{2,1,0:T(8,128)S(1)}, f32[4,8,32,1]{2,1,3,0:T(8,...) while((s32[]{:T(128)}, f32[8,32,64]{2,1,0:T(8,128)S(1)}, ...), condition=%wide.region_12.13_spmd, body=%wide.region_11.12_spmd.sunk | while | flops 32770 | bytes 477293 | solution.py:51
  213.3 2.4 convert_reduce_fusion
  217.6 3.1 fusion.20
  221.4 5.0 %fusion.6 = bf16[1,2048,512]{2,1,0:T(8,128)(2,1)} fusion(bf16[640,2048]{1,0:T(8,128)(2,1)} %all-gather.6.cloned.1.call-done, bf16[640,512]{1,0:T(8,128)(2,1)S(1)} %copy-done.28), kind=kOutput, calls=%fused_computation.28 | convolution fusion | flops 1343225856 | bytes 5373952 | tf_op jit(solution)/shard_map/dot_general | solution.py:164
  226.5 3.2 fusion.7
  229.6 4.9 %fusion.8 = bf16[1,512,2048]{2,1,0:T(8,128)(2,1)} fusion(bf16[640,2048]{0,1:T(8,128)(2,1)} %bitcast.13, f32[640,512]{1,0:T(8,128)S(1)} %copy-done.51, f32[640,512]{1,0:T(8,128)S(1)} %copy-done.50), kind=kOutput, calls=%fused_computation.30 | convolution fusion | flops 1345191936 | bytes 7340032 | tf_op jit(solution)/shard_map/dot_general | solution.py:157
  234.6 9.9 %all-gather.8.cloned.1.call-done = bf16[256,2048]{1,0:T(8,128)(2,1)} async-done(((bf16[256,512]{1,0:T(8,128)(2,1)}), bf16[256,2048]{1,0:T(8,128)(2,1)}) %all-gather.8.cloned.1.call-update) | async-done | bytes 1048592 | tf_op jit(solution)/shard_map/all_gather | solution.py:187
  244.5 3.3 convolution_convert_fusion
  254.1 2.5 fusion.27
  257.6 12.7 %while.65 = (s32[]{:T(128)}, f32[8,32,64]{2,1,0:T(8,128)S(1)}, f32[4,8,32]{2,1,0:T(8,128)S(1)}, f32[4,8,32,64]{3,2,1,0:T(8,128)}, f32[4,8,32,64]{3,2,1,0:T(8,128...) while((s32[]{:T(128)}, f32[8,32,64]{2,1,0:T(8,128)S(1)}, ...), condition=%wide.region_16.17_spmd.clone, body=%wide.region_14.16_spmd.clone.sunk | while | flops 98308 | bytes 472220 | solution.py:51
  270.3 2.8 fusion.41
  273.0 19.8 %all-gather.2 = f32[64,32,64]{2,1,0:T(8,128)} all-gather(f32[8,32,64]{2,1,0:T(8,128)S(1)} %get-tuple-element.402), channel_id=4, replica_groups=mesh['sp'=8,'tp'=4] {'sp'}, dimensions={0}, use_global_device_ids=true | all-gather | bytes 589824 | tf_op jit(solution)/shard_map/all_gather | solution.py:15
  295.1 12.5 %while.66 = (s32[]{:T(128)}, f32[8,32,64]{2,1,0:T(8,128)S(1)}, s32[]{:T(128)}, f32[8,8,32]{2,1,0:T(8,128)}, f32[8,8,32,64]{3,2,1,0:T(8,128)}, /*index=5*/s32[]{:T(128)}, s32[]{:T(128)}) while((s32[]{:T(128)}, f32[8,32,64]{2,1,0:T(8,128)S(1)}, s32[]{:T(128)}, f32[8,8,32]{2,1,0:T(8,128)}, f32[8,8,32,64]{3,2,1,0:T(8,128)}, ...), condition=%wide.region_18.19_spmd.clone, body=%wide.region_17.18_spmd.clone.sunk | while | flops 65540 | bytes 199793 | solution.py:27
  313.9 2.9 pad_add_fusion.1
  335.8 25.7 %fusion.67 = f32[4,64,8,32]{3,2,1,0:T(8,128)S(1)} fusion(f32[4,64,8,32]{3,2,1,0:T(8,128)S(1)} %copy.148), kind=kOutput, calls=%fused_computation.147 | output fusion | flops 4128768 | bytes 524288 | tf_op jit(solution)/shard_map/transpose(jvp(jit(cumsum)))/reduce_window_sum | solution.py:38
  361.5 25.8 %fusion.68 = f32[4,64,8,32]{3,2,1,0:T(8,128)S(1)} fusion(f32[4,64,8,32]{3,2,1,0:T(8,128)S(1)} %copy-done.16), kind=kOutput, calls=%fused_computation.148 | output fusion | flops 4128768 | bytes 524288 | tf_op jit(solution)/shard_map/transpose(jvp(jit(cumsum)))/reduce_window_sum | solution.py:62
  (280 shorter events, 111.9 us)
Async XLA Ops:
  7.2 89.6 %copy-start = (bf16[1,2048,512]{2,1,0:T(8,128)(2,1)S(1)}, bf16[1,2048,512]{2,1,0:T(8,128)(2,1)}, u32[]{:S(2)}) copy-start(bf16[1,2048,512]{2,1,0:T(8,128)(2,1)} %param.24) | copy-start | bytes 6291460
  7.2 89.6 %all-gather.6.cloned.1.call-start = ((), (), s32[]{:S(2)}) async-start(), calls=%async_computation.6 | async-start | bytes 3276800 | tf_op jit(solution)/shard_map/all_gather | solution.py:138
  17.9 24.6 %copy-start.26 = (bf16[256,512]{1,0:T(8,128)(2,1)S(1)}, bf16[256,512]{1,0:T(8,128)(2,1)}, u32[]{:S(2)}) copy-start(bf16[256,512]{1,0:T(8,128)(2,1)} %param.21) | copy-start | bytes 786436
  71.8 37.2 %all-to-all-start.2 = ((bf16[4,640,512]{1,2,0:T(8,128)(2,1)}), bf16[4,640,512]{1,2,0:T(8,128)(2,1)}, u32[]{:S(2)}, u32[]{:S(2)}) async-start(bf16[4,640,512]{1,2,0:T(8,128)(2,1)} %stack.3), calls=%async_computation.2 | async-start | bytes 5242880 | tf_op jit(solution)/shard_map/all_to_all | solution.py:140
  76.3 109.8 %reduce-scatter.3.cloned.1.call-start = ((), (), s32[]{:S(2)}) async-start(), calls=%async_computation.7 | async-start | bytes 3276800 | tf_op jit(solution)/shard_map/reduce_scatter | solution.py:176
  96.8 3.4 copy-start.20
  96.8 3.4 copy-start.47
  100.2 8.7 %copy-start.49 = (f32[640,512]{1,0:T(8,128)}, f32[640,512]{1,0:T(8,128)S(1)}, u32[]{:S(2)}) copy-start(f32[640,512]{1,0:T(8,128)S(1)} %fusion.11) | copy-start | bytes 3932164
  120.4 26.3 %copy-start.39 = (bf16[256,256]{1,0:T(8,128)(2,1)S(1)}, bf16[256,256]{1,0:T(8,128)(2,1)}, u32[]{:S(2)}) copy-start(bf16[256,256]{1,0:T(8,128)(2,1)} %param.28) | copy-start | bytes 393220
  146.6 59.2 %copy-start.2 = (f32[4,64,8,32]{1,3,2,0:T(8,128)}, f32[4,64,8,32]{1,3,2,0:T(8,128)S(1)}, u32[]{:S(2)}) copy-start(f32[4,64,8,32]{1,3,2,0:T(8,128)S(1)} %copy.125) | copy-start | bytes 786436
  147.5 17.6 %copy-start.12 = (f32[4,64,8,32]{1,0,3,2:T(4,128)}, f32[4,64,8,32]{1,0,3,2:T(4,128)S(1)}, u32[]{:S(2)}) copy-start(f32[4,64,8,32]{1,0,3,2:T(4,128)S(1)} %reshape.248) | copy-start | bytes 786436
  148.6 16.6 %copy-start.41 = (f32[8,32]{1,0:T(8,128)}, f32[8,32]{1,0:T(8,128)S(1)}, u32[]{:S(2)}) copy-start(f32[8,32]{1,0:T(8,128)S(1)} %get-tuple-element.558) | copy-start | bytes 3076
  149.3 15.8 %copy-start.31 = (f32[4,8,32]{2,1,0:T(8,128)}, f32[4,8,32]{2,1,0:T(8,128)S(1)}, u32[]{:S(2)}) copy-start(f32[4,8,32]{2,1,0:T(8,128)S(1)} %fusion.25) | copy-start | bytes 12292
  186.1 5.1 %copy-start.10 = (f32[8,32,64]{2,1,0:T(8,128)}, f32[8,32,64]{2,1,0:T(8,128)S(1)}, u32[]{:S(2)}) copy-start(f32[8,32,64]{2,1,0:T(8,128)S(1)} %get-tuple-element.750) | copy-start | bytes 196612
  186.2 24.9 %all-to-all-start.3 = ((bf16[8,80,512]{2,1,0:T(8,128)(2,1)}), bf16[8,80,512]{2,1,0:T(8,128)(2,1)S(1)}, u32[]{:S(2)}, u32[]{:S(2)}) async-start(bf16[8,80,512]{2,1,0:T(8,128)(2,1)} %bitcast.211), calls=%async_computation.4 | async-start | bytes 1310720 | tf_op jit(solution)/shard_map/all_to_all | solution.py:179
  191.2 6.9 %copy-start.44 = (s32[512]{0:T(512)S(1)}, s32[512]{0:T(512)}, u32[]{:S(2)}) copy-start(s32[512]{0:T(512)} %copy-done.43) | copy-start | bytes 6148
  191.2 53.3 %all-gather.8.cloned.1.call-start = ((), (), s32[]{:S(2)}) async-start(), calls=%async_computation.8 | async-start | bytes 1310720 | tf_op jit(solution)/shard_map/all_gather | solution.py:187
  198.1 19.5 %copy-start.4 = (f32[4,8,32,64]{3,2,1,0:T(8,128)}, f32[4,8,32,64]{3,2,1,0:T(8,128)S(1)}, u32[]{:S(2)}) copy-start(f32[4,8,32,64]{3,2,1,0:T(8,128)S(1)} %get-tuple-element.779) | copy-start | bytes 786436
  217.5 170.9 %reduce-scatter.5.cloned.1.call-start = ((), (), s32[]{:S(2)}) async-start(), calls=%async_computation.9 | async-start | bytes 2359296 | tf_op jit(solution)/shard_map/reduce_scatter | solution.py:188
  217.6 3.8 copy-start.28
  221.4 5.1 %copy-start.30 = (bf16[640,512]{1,0:T(8,128)(2,1)S(1)}, bf16[640,512]{1,0:T(8,128)(2,1)}, u32[]{:S(2)}) copy-start(bf16[640,512]{1,0:T(8,128)(2,1)} %copy-done.29) | copy-start | bytes 1966084
  221.4 5.1 %copy-start.48 = (bf16[640,2048]{1,0:T(8,128)(2,1)S(1)}, bf16[640,2048]{1,0:T(8,128)(2,1)}, u32[]{:S(2)}) copy-start(bf16[640,2048]{1,0:T(8,128)(2,1)} %all-gather.6.cloned.1.call-done) | copy-start | bytes 7864324
  257.6 12.7 %copy-start.3 = (f32[4,64,8,32]{1,3,2,0:T(8,128)S(1)}, f32[4,64,8,32]{1,3,2,0:T(8,128)}, u32[]{:S(2)}) copy-start(f32[4,64,8,32]{1,3,2,0:T(8,128)} %copy-done.2) | copy-start | bytes 786436
  292.8 15.8 %copy-start.32 = (f32[4,8,32]{2,1,0:T(8,128)S(1)}, f32[4,8,32]{2,1,0:T(8,128)}, u32[]{:S(2)}) copy-start(f32[4,8,32]{2,1,0:T(8,128)} %copy-done.31) | copy-start | bytes 12292
  307.6 4.2 %copy-start.34 = (f32[64,64]{1,0:T(8,128)S(1)}, f32[64,64]{1,0:T(8,128)}, u32[]{:S(2)}) copy-start(f32[64,64]{1,0:T(8,128)} %copy-done.33) | copy-start | bytes 49156
  316.8 6.8 %copy-start.9 = (f32[4,64,8,32]{1,3,2,0:T(8,128)S(1)}, f32[4,64,8,32]{1,3,2,0:T(8,128)}, u32[]{:S(2)}) copy-start(f32[4,64,8,32]{1,3,2,0:T(8,128)} %copy-done.8) | copy-start | bytes 786436
  316.8 6.8 %copy-start.14 = (f32[4,8,32,64]{3,2,1,0:T(8,128)S(1)}, f32[4,8,32,64]{3,2,1,0:T(8,128)}, u32[]{:S(2)}) copy-start(f32[4,8,32,64]{3,2,1,0:T(8,128)} %get-tuple-element.401) | copy-start | bytes 786436
  317.7 7.8 %copy-start.7 = (f32[4,8,64,64]{3,2,1,0:T(8,128)S(1)}, f32[4,8,64,64]{3,2,1,0:T(8,128)}, u32[]{:S(2)}) copy-start(f32[4,8,64,64]{3,2,1,0:T(8,128)} %copy-done.6) | copy-start | bytes 1572868
  326.7 3.6 copy-start.23
  330.7 3.5 copy-start.22
  335.8 25.7 %copy-start.16 = (f32[4,64,8,32]{3,2,1,0:T(8,128)S(1)}, f32[4,64,8,32]{3,2,1,0:T(8,128)}, u32[]{:S(2)}) copy-start(f32[4,64,8,32]{3,2,1,0:T(8,128)} %copy.152) | copy-start | bytes 786436
  361.5 28.7 %copy-start.1 = (bf16[1,2048,512]{2,1,0:T(8,128)(2,1)S(1)}, bf16[1,2048,512]{2,1,0:T(8,128)(2,1)}, u32[]{:S(2)}) copy-start(bf16[1,2048,512]{2,1,0:T(8,128)(2,1)} %param.24) | copy-start | bytes 6291460
  (26 other events, 46.9 us)
Sparse Core Ops, SparseCore 0:
  42.6 54.1 all-gather.5
  118.9 39.5 reduce-scatter.2
  217.6 26.8 all-gather.7
  248.0 36.9 reduce-scatter.4
